TPU v7x, 32 devices: a whole 2x2x4 slice. The times are simulated.
32 devices in a mesh: sp: 4 (over y, x), tp: 8 (over z, core).
Axes of the slice: x: 2, y: 2, z: 4, core: 2. Of those that a mesh axis runs over, the one named last changes fastest.
Arguments:
- cotangent: bfloat16 [1024, 2048], P('sp', 'tp'), may hold values from -6 to 6
- block_input: bfloat16 [1024, 2048], P('sp', 'tp'), may hold values from -6 to 6
- routes: int32 [1024, 2], P('sp'), may hold values from 0 to 3, all different within a row; in each aligned block of 256 rows (0 to 255, 256 to 511, ...) at most 160 rows name the same one
- route_weights: float32 [1024, 2], P('sp'), may hold values from 0.1 to 0.9
- gate_weight: bfloat16 [4, 2048, 7168], P('sp', None, 'tp'), may hold values from -0.125 to 0.125
- up_weight: bfloat16 [4, 2048, 7168], P('sp', None, 'tp'), may hold values from -0.125 to 0.125
- down_weight: bfloat16 [4, 7168, 2048], P('sp', 'tp'), may hold values from -0.0625 to 0.0625
- out_weight: bfloat16 [1024, 2048], P('tp'), may hold values from -0.1875 to 0.1875
- conv_out: bfloat16 [1024, 1024], P('tp', 'sp'), may hold values from -6 to 6
- gate_pre: bfloat16 [1024, 1024], P('tp', 'sp'), may hold values from -6 to 6
- prior_states: bfloat16 [1024, 1024], P('tp', 'sp'), may hold values from -6 to 6
- recur_weight: bfloat16 [16, 64, 64], replicated, may hold values from -0.75 to 0.75
- input_gate_matrix: bfloat16 [16, 64, 64], replicated, may hold values from -0.75 to 0.75
- decay_param: float32 [1024], replicated, may hold values from 4 to 16
- decay_jump: float32 [1024, 1024], P('tp', 'sp'), may hold values from -1 to 0, as said below
Outputs:
- gate_weight_grad: bfloat16 [4, 2048, 7168], P('sp', None, 'tp')
- up_weight_grad: bfloat16 [4, 2048, 7168], P('sp', None, 'tp')
- down_weight_grad: bfloat16 [4, 7168, 2048], P('sp', 'tp')
- out_weight_grad: float32 [1024, 2048], P('tp', 'sp')
- conv_grad: bfloat16 [1024, 1024], P('tp', 'sp')
- valve_logit_derivative: bfloat16 [1024, 1024], P('tp', 'sp')
Inputs may be any that keep to these rules, and one draw needn't show every extreme that they name: In each aligned block of 256 rows (the rows of one index of sp) no expert is named by more than 160 routes, a bound that some block reaches; a row names 2 different experts. `decay_jump`: every entry is at most -1 / 20480.
All inputs are finite; a program needn't handle non-finite values.
Results may differ from a plain program's by a relative error of at most 0.018.
Values may be sent and summed in bfloat16 or wider, within the bound.
A program may use at most 128 MiB of HBM per device.

v0:
```python
import jax
import jax.numpy as jnp
from jax import lax
from jax.sharding import PartitionSpec as P

HEAD_DIM = 64
TOP_K = 2
RATE_SCALE = 8.0


def prefix(value, axis, join, neutral):
    count, mine = (lax.axis_size(axis), lax.axis_index(axis))
    pieces = jax.tree.map(lambda part: lax.all_gather(part, axis), value)
    pieces = jax.tree.map(lambda part: part[::-1], pieces)
    mine = count - 1 - mine
    so_far = jax.tree.map(
        lambda part, zero: jnp.full_like(part, 0) + jnp.asarray(zero, part.dtype), value, neutral
    )

    def turn(position, so_far):
        longer = join(so_far, jax.tree.map(lambda part: part[position], pieces))
        return jax.tree.map(lambda new, old: jnp.where(position < mine, new, old), longer, so_far)

    return lax.fori_loop(0, count - 1, turn, so_far)


def link_pairs(left_pair, right_pair):
    return (left_pair[0] * right_pair[0], right_pair[0] * left_pair[1] + right_pair[1])


def later_first(earlier_pair, later_pair):
    return (earlier_pair[0] * later_pair[0], later_pair[1] + later_pair[0] * earlier_pair[1])


def routing_tables(routes, experts, capacity):
    flat_routes = routes.reshape(-1)
    onehot = (flat_routes[:, None] == jnp.arange(experts, dtype=jnp.int32)[None, :]).astype(
        jnp.int32
    )
    slot_rank = jnp.sum((jnp.cumsum(onehot, axis=0) - onehot) * onehot, axis=1)
    target = (flat_routes * capacity + slot_rank).reshape(routes.shape[0], routes.shape[1])
    slot_ids = jnp.arange(experts * capacity, dtype=jnp.int32)
    return jnp.transpose(target)[:, None, :] == slot_ids[None, :, None]


def spread(placing, route_hits, rows_in, cot_in, route_weights):
    sent_rows = jnp.dot(placing, rows_in, preferred_element_type=jnp.float32).astype(jnp.bfloat16)
    scaled = (
        jnp.transpose(route_weights)[:, :, None] * cot_in.astype(jnp.float32)[None, :, :]
    ).astype(jnp.bfloat16)
    sent_cot = jnp.einsum(
        "kst,ktd->sd", route_hits, scaled, preferred_element_type=jnp.float32
    ).astype(jnp.bfloat16)
    return (sent_rows, sent_cot)


def expert_work(slot_rows, slot_cot, w_gate, w_up, w_down):
    minor = (((1,), (1,)), ((), ()))
    gate_act = jnp.dot(slot_rows, w_gate, preferred_element_type=jnp.float32)
    up_act = jnp.dot(slot_rows, w_up, preferred_element_type=jnp.float32)
    sigma_gate = jax.nn.sigmoid(gate_act)
    silu_val = gate_act * sigma_gate
    hidden = (silu_val * up_act).astype(jnp.bfloat16)
    d_hidden = lax.dot_general(slot_cot, w_down, minor, preferred_element_type=jnp.float32)
    d_gate = (d_hidden * up_act * sigma_gate * (1.0 + gate_act * (1.0 - sigma_gate))).astype(
        jnp.bfloat16
    )
    d_up = (d_hidden * silu_val).astype(jnp.bfloat16)
    width_part = lax.dot_general(d_gate, w_gate, minor, preferred_element_type=jnp.float32)
    width_part = width_part + lax.dot_general(d_up, w_up, minor, preferred_element_type=jnp.float32)
    return (hidden, d_gate, d_up, width_part)


def weight_grads(slot_rows, slot_cot, hidden, d_gate, d_up):
    major = (((0,), (0,)), ((), ()))
    gate_grad = lax.dot_general(
        slot_rows, d_gate, major, preferred_element_type=jnp.float32
    ).astype(jnp.bfloat16)
    up_grad = lax.dot_general(slot_rows, d_up, major, preferred_element_type=jnp.float32).astype(
        jnp.bfloat16
    )
    down_grad = lax.dot_general(hidden, slot_cot, major, preferred_element_type=jnp.float32).astype(
        jnp.bfloat16
    )
    return (gate_grad[None], up_grad[None], down_grad[None])


def local(
    cotangent,
    block_input,
    routes,
    route_weights,
    gate_weight,
    up_weight,
    down_weight,
    out_weight,
    conv_out,
    gate_pre,
    prior_states,
    recur_weight,
    input_gate_matrix,
    decay_param,
    decay_jump,
):
    experts = lax.axis_size("sp")
    tok_rows = cotangent.shape[0]
    capacity = 5 * tok_rows * TOP_K // (4 * experts)
    route_hits = routing_tables(routes, experts, capacity)
    placing = jnp.sum(route_hits.astype(jnp.int32), axis=0).astype(jnp.bfloat16)
    hit_table = route_hits.astype(jnp.bfloat16)
    sent_rows, sent_cot = spread(placing, hit_table, block_input, cotangent, route_weights)
    part_rows, portion_adjoint = (
        lax.all_to_all(
            sent_rows.reshape(experts, capacity, -1), "sp", split_axis=0, concat_axis=0, tiled=True
        ),
        lax.all_to_all(
            sent_cot.reshape(experts, capacity, -1), "sp", split_axis=0, concat_axis=0, tiled=True
        ),
    )
    got_rows, got_cot = (
        lax.all_gather(part_rows, "tp", axis=2, tiled=True),
        lax.all_gather(portion_adjoint, "tp", axis=2, tiled=True),
    )
    full_width = got_rows.shape[2]
    slot_rows = got_rows.reshape(-1, full_width)
    slot_cot = got_cot.reshape(-1, full_width)
    hidden, d_gate, d_up, width_part = expert_work(
        slot_rows, slot_cot, gate_weight[0], up_weight[0], down_weight[0]
    )
    gate_grad, up_grad, down_grad = weight_grads(slot_rows, slot_cot, hidden, d_gate, d_up)
    summed = lax.psum_scatter(
        width_part.reshape(experts, capacity, full_width).astype(jnp.bfloat16),
        "tp",
        scatter_dimension=2,
        tiled=True,
    )
    handed_result = lax.all_to_all(summed, "sp", split_axis=0, concat_axis=0, tiled=True).reshape(
        experts * capacity, -1
    )
    moe_grad = lax.dot_general(
        placing, handed_result, (((0,), (0,)), ((), ())), preferred_element_type=jnp.float32
    )
    block_grad = (cotangent.astype(jnp.float32) + moe_grad).astype(jnp.bfloat16)
    full_grad = lax.all_gather(block_grad, "tp", axis=1, tiled=True)
    channels = conv_out.shape[0]
    length = conv_out.shape[1]
    head_count = channels // HEAD_DIM
    head_start = lax.axis_index("tp") * head_count
    w_recur = lax.dynamic_slice_in_dim(recur_weight, head_start, head_count, 0)
    w_input = lax.dynamic_slice_in_dim(input_gate_matrix, head_start, head_count, 0)
    rate_parameter = lax.dynamic_slice_in_dim(decay_param, head_start * HEAD_DIM, channels, 0)[
        :, None
    ]
    shaped = conv_out.reshape(head_count, HEAD_DIM, length)
    recur_gate = jax.nn.sigmoid(
        jnp.einsum("hij,hit->hjt", w_recur, shaped, preferred_element_type=jnp.float32).reshape(
            channels, length
        )
    )
    input_gate = jax.nn.sigmoid(
        jnp.einsum("hij,hit->hjt", w_input, shaped, preferred_element_type=jnp.float32).reshape(
            channels, length
        )
    )
    softened = jax.nn.softplus(-rate_parameter)
    log_decay = -RATE_SCALE * recur_gate * softened + decay_jump
    decay_val = jnp.exp(log_decay)
    norm_scale = jnp.sqrt(-jnp.expm1(2.0 * log_decay))
    conv_vals = conv_out.astype(jnp.float32)
    prior_vals = prior_states.astype(jnp.float32)
    state = decay_val * prior_vals + norm_scale * input_gate * conv_vals
    gelu_val, gelu_pull = jax.vjp(jax.nn.gelu, gate_pre.astype(jnp.float32))
    mixed = (gelu_val * state).astype(jnp.bfloat16)
    d_mixed = lax.dot_general(
        out_weight, full_grad, (((1,), (1,)), ((), ())), preferred_element_type=jnp.float32
    )
    valve_logit_derivative = gelu_pull(d_mixed * state)[0].astype(jnp.bfloat16)
    d_state = d_mixed * gelu_val
    shifted = jnp.concatenate([decay_val[:, 1:], jnp.ones((channels, 1), jnp.float32)], axis=1)
    flipped = lax.associative_scan(link_pairs, (jnp.flip(shifted, 1), jnp.flip(d_state, 1)), axis=1)
    decay_prod = jnp.flip(flipped[0], 1)
    local_sum = jnp.flip(flipped[1], 1)
    summary = (decay_val[:, 0] * decay_prod[:, 0], decay_val[:, 0] * local_sum[:, 0])
    carried = prefix(
        summary,
        "sp",
        later_first,
        (jnp.ones((channels,), jnp.float32), jnp.zeros((channels,), jnp.float32)),
    )[1]
    state_grad = local_sum + decay_prod * carried[:, None]
    grad_log = (
        state_grad * prior_vals * decay_val
        - state_grad * input_gate * conv_vals * decay_val * decay_val / norm_scale
    )
    grad_recur = (grad_log * -RATE_SCALE * softened * recur_gate * (1.0 - recur_gate)).astype(
        jnp.bfloat16
    )
    grad_input = (state_grad * norm_scale * conv_vals * input_gate * (1.0 - input_gate)).astype(
        jnp.bfloat16
    )
    back_recur = jnp.einsum(
        "hij,hjt->hit",
        w_recur,
        grad_recur.reshape(head_count, HEAD_DIM, length),
        preferred_element_type=jnp.float32,
    ).reshape(channels, length)
    back_input = jnp.einsum(
        "hij,hjt->hit",
        w_input,
        grad_input.reshape(head_count, HEAD_DIM, length),
        preferred_element_type=jnp.float32,
    ).reshape(channels, length)
    conv_grad = (state_grad * norm_scale * input_gate + back_recur + back_input).astype(
        jnp.bfloat16
    )
    projected = lax.psum_scatter(
        lax.dot_general(
            full_grad, mixed, (((0,), (1,)), ((), ())), preferred_element_type=jnp.float32
        ).astype(jnp.bfloat16),
        "sp",
        scatter_dimension=0,
        tiled=True,
    ).astype(jnp.float32)
    out_weight_grad = jnp.transpose(projected)
    return (gate_grad, up_grad, down_grad, out_weight_grad, conv_grad, valve_logit_derivative)


def solution(mesh):
    in_specs = (
        P("sp", "tp"),
        P("sp", "tp"),
        P("sp", None),
        P("sp", None),
        P("sp", None, "tp"),
        P("sp", None, "tp"),
        P("sp", "tp", None),
        P("tp", None),
        P("tp", "sp"),
        P("tp", "sp"),
        P("tp", "sp"),
        P(),
        P(),
        P(),
        P("tp", "sp"),
    )
    out_specs = (
        P("sp", None, "tp"),
        P("sp", None, "tp"),
        P("sp", "tp", None),
        P("tp", "sp"),
        P("tp", "sp"),
        P("tp", "sp"),
    )
    return jax.shard_map(local, mesh=mesh, in_specs=in_specs, out_specs=out_specs, check_vma=False)
```

profile of v0, /device:TPU:0, one launch (start us, length us, event | category | flops | bytes accessed | tf_op | source)
XLA Modules:
  0.0 229.2 jit_solution(16892057116044407689)
XLA Ops:
  7.2 0.0 all-gather.6.cloned.1.call-start
  7.2 0.9 copy.72
  8.1 0.1 eq.42
  8.3 0.1 eq.38
  8.4 1.2 reduce-window.6
  9.7 0.2 slice_reduce_fusion
  9.9 0.2 reduce-window.9
  10.1 0.1 add_bitcast_fusion
  10.2 0.1 reduce_sum.21
  10.3 0.1 copy.74
  10.4 0.7 add_bitcast_fusion.1
  11.1 0.3 convert_reduce_fusion
  11.3 1.1 convolution_convert_fusion.1
  12.5 11.7 %all_to_all.15 = bf16[4,160,256]{2,1,0:T(8,128)(2,1)} all-to-all(bf16[4,160,256]{2,1,0:T(8,128)(2,1)S(1)} %bitcast.101), channel_id=1, replica_groups=mesh['sp'=4,'tp'=8] {'sp'}, dimensions={0} | all-to-all | bytes 655360 | tf_op jit(solution)/shard_map/all_to_all | solution.py:113
  24.2 0.0 all-gather.8.cloned.1.call-start
  24.3 0.5 fusion.16
  24.8 9.3 %all_to_all.16 = bf16[4,160,256]{2,1,0:T(8,128)(2,1)} all-to-all(bf16[4,160,256]{2,1,0:T(8,128)(2,1)S(1)} %bitcast.104), channel_id=1, replica_groups=mesh['sp'=4,'tp'=8] {'sp'}, dimensions={0} | all-to-all | bytes 655360 | tf_op jit(solution)/shard_map/all_to_all | solution.py:116
  34.1 0.0 reduce-scatter.3.cloned.1.call-start
  34.2 24.6 %all-gather.6.cloned.1.call-done = bf16[4,160,2048]{2,1,0:T(8,128)(2,1)} async-done(((bf16[4,160,256]{2,1,0:T(8,128)(2,1)}), bf16[4,160,2048]{2,1,0:T(8,128)(2,1)}) %all-gather.6.cloned.1.call-update) | async-done | bytes 2621456 | tf_op jit(solution)/shard_map/all_gather | solution.py:121
  58.8 7.2 %fusion.3 = f32[640,896]{1,0:T(8,128)} fusion(bf16[640,2048]{1,0:T(8,128)(2,1)} %bitcast.114, bf16[1,2048,896]{2,1,0:T(8,128)(2,1)} %param.21), kind=kOutput, calls=%fused_computation.7 | convolution fusion | flops 2348810240 | bytes 8585216 | tf_op jit(solution)/shard_map/dot_general | solution.py:59
  66.0 4.3 %fusion.7 = f32[640,896]{1,0:T(8,128)} fusion(bf16[640,2048]{1,0:T(8,128)(2,1)S(1)} %bitcast.116, bf16[1,2048,896]{2,1,0:T(8,128)(2,1)S(1)} %copy-done.8), kind=kOutput, calls=%fused_computation.11 | convolution fusion | flops 2348810240 | bytes 8585216 | tf_op jit(solution)/shard_map/dot_general | solution.py:60
  70.4 23.2 %all-gather.8.cloned.1.call-done = bf16[4,160,2048]{2,1,0:T(8,128)(2,1)} async-done(((bf16[4,160,256]{2,1,0:T(8,128)(2,1)}), bf16[4,160,2048]{2,1,0:T(8,128)(2,1)}) %all-gather.8.cloned.1.call-update) | async-done | bytes 2621456 | tf_op jit(solution)/shard_map/all_gather | solution.py:122
  93.6 7.8 %multiply_convert_fusion.1 = (bf16[640,896]{1,0:T(8,128)(2,1)S(1)}, bf16[640,896]{1,0:T(8,128)(2,1)S(1)}) fusion(f32[640,896]{1,0:T(8,128)} %fusion.3, f32[640,896]{1,0:T(8,128)} %fusion.7, bf16[640,2048]{1,0:T(8,128)(2,1)} %bitcast.118, bf16[1,896,2048]{2,1,0:T(8,128)(2,1)} %param.23), kind=kOutput, calls=%fused_computation.20 | convolution fusion | flops 2356264960 | bytes 13172736 | tf_op jit(solution)/shard_map/dot_general | solution.py:64
  101.5 2.9 %fusion.1 = f32[640,2048]{1,0:T(8,128)S(1)} fusion(bf16[640,896]{1,0:T(8,128)(2,1)S(1)} %get-tuple-element.152, bf16[1,2048,896]{2,1,0:T(8,128)(2,1)S(1)} %copy-done.7), kind=kOutput, calls=%fused_computation.5 | convolution fusion | flops 2348810240 | bytes 10059776 | tf_op jit(solution)/shard_map/dot_general | solution.py:69
  104.4 4.2 %add_convert_fusion = bf16[640,2048]{1,0:T(8,128)(2,1)} fusion(f32[640,2048]{1,0:T(8,128)S(1)} %fusion.1, bf16[640,896]{1,0:T(8,128)(2,1)S(1)} %get-tuple-element.151, bf16[1,2048,896]{2,1,0:T(8,128)(2,1)S(1)} %copy-done.9), kind=kOutput, calls=%fused_computation.4 | convolution fusion | flops 2351431680 | bytes 12681216 | tf_op jit(solution)/shard_map/dot_general | solution.py:70
  108.6 0.8 copy-done.4
  109.4 0.1 copy.82
  109.5 1.0 fusion.23
  110.6 0.1 copy.81
  110.7 34.2 %reduce-scatter.3.cloned.1.call-done = bf16[4,160,256]{2,1,0:T(8,128)(2,1)} async-done(((bf16[4,160,2048]{2,1,0:T(8,128)(2,1)}), bf16[4,160,256]{2,1,0:T(8,128)(2,1)}) %reduce-scatter.3.cloned.1.call-update) | async-done | bytes 327696 | tf_op jit(solution)/shard_map/reduce_scatter | solution.py:131
  144.9 3.7 %all-to-all-start.2 = ((bf16[4,160,256]{2,1,0:T(8,128)(2,1)}), bf16[4,160,256]{2,1,0:T(8,128)(2,1)S(1)}, u32[]{:S(2)}, u32[]{:S(2)}) async-start(bf16[4,160,256]{2,1,0:T(8,128)(2,1)} %reduce-scatter.3.cloned.1.call-done), calls=%async_computation.3 | async-start | bytes 655360 | tf_op jit(solution)/shard_map/all_to_all | solution.py:137
  148.5 0.0 all-gather.10.cloned.1.call-start
  148.6 1.0 fusion.21
  149.6 0.1 copy.77
  149.7 0.1 copy.79
  149.8 0.1 copy.75
  149.9 0.1 copy.78
  150.0 0.8 fusion.70
  150.8 3.3 %all-to-all-done.2 = bf16[4,160,256]{2,1,0:T(8,128)(2,1)S(1)} async-done(((bf16[4,160,256]{2,1,0:T(8,128)(2,1)}), bf16[4,160,256]{2,1,0:T(8,128)(2,1)S(1)}, u32[]{:S(2)}, u32[]{:S(2)}) %all-to-all-start.2) | async-done | bytes 327712 | tf_op jit(solution)/shard_map/all_to_all | solution.py:137
  154.1 1.0 fusion.17
  155.1 0.0 reduce-scatter.5.cloned.1.call-start
  155.1 7.4 %convert_bitcast_fusion.1 = bf16[1,2048,896]{2,1,0:T(8,128)(2,1)} fusion(bf16[640,2048]{1,0:T(8,128)(2,1)} %bitcast.115, bf16[640,896]{1,0:T(8,128)(2,1)} %copy-done.18), kind=kOutput, calls=%fused_computation.16 | convolution fusion | flops 2350645248 | bytes 7438336 | tf_op jit(solution)/shard_map/dot_general | solution.py:79
  162.6 4.9 %convert_bitcast_fusion.2 = bf16[1,2048,896]{2,1,0:T(8,128)(2,1)} fusion(bf16[640,2048]{1,0:T(8,128)(2,1)S(1)} %bitcast.117, bf16[640,896]{1,0:T(8,128)(2,1)S(1)} %copy-done.15), kind=kOutput, calls=%fused_computation.17 | convolution fusion | flops 2350645248 | bytes 7438336 | tf_op jit(solution)/shard_map/dot_general | solution.py:76
  167.5 4.6 %convert_bitcast_fusion = bf16[1,896,2048]{2,1,0:T(8,128)(2,1)} fusion(bf16[640,2048]{1,0:T(8,128)(2,1)S(1)} %bitcast.119, f32[640,896]{1,0:T(8,128)S(1)} %copy-done.17, f32[640,896]{1,0:T(8,128)S(1)} %copy-done.16), kind=kOutput, calls=%fused_computation.15 | convolution fusion | flops 2354085888 | bytes 10878976 | tf_op jit(solution)/shard_map/dot_general | solution.py:82
  172.1 4.3 %all-gather.10.cloned.1.call-done = bf16[256,2048]{1,0:T(8,128)(2,1)} async-done(((bf16[256,256]{1,0:T(8,128)(2,1)}), bf16[256,2048]{1,0:T(8,128)(2,1)}) %all-gather.10.cloned.1.call-update) | async-done | bytes 1048592 | tf_op jit(solution)/shard_map/all_gather | solution.py:144
  176.4 1.7 fusion.40
  180.3 7.2 %all-gather = f32[512,1]{0,1:T(1,128)S(1)} all-gather(f32[128,1]{0,1:T(1,128)S(1)} %get-tuple-element.156), channel_id=2, replica_groups=mesh['sp'=4,'tp'=8] {'sp'}, dimensions={0}, use_global_device_ids=true | all-gather | bytes 2560 | tf_op jit(solution)/shard_map/all_gather | solution.py:13
  187.5 7.9 %all-gather.1 = f32[512,1]{0,1:T(1,128)S(1)} all-gather(f32[128,1]{0,1:T(1,128)S(1)} %get-tuple-element.155), channel_id=3, replica_groups=mesh['sp'=4,'tp'=8] {'sp'}, dimensions={0}, use_global_device_ids=true | all-gather | bytes 2560 | tf_op jit(solution)/shard_map/all_gather | solution.py:13
  195.4 1.4 convolution_convert_fusion
  196.8 0.1 while.14
  197.0 0.1 rev.16
  197.1 0.1 rev.15
  197.2 0.2 fusion.43
  197.4 0.1 copy.87
  197.5 0.9 fusion.62
  198.4 0.1 copy.89
  198.5 0.1 copy.92
  198.6 0.9 fusion.59
  199.5 0.1 copy.94
  199.7 0.7 copy.96
  200.4 0.7 copy.97
  201.1 19.8 %reduce-scatter.5.cloned.1.call-done = bf16[512,128]{1,0:T(8,128)(2,1)} async-done(((bf16[2048,128]{1,0:T(8,128)(2,1)}), bf16[512,128]{1,0:T(8,128)(2,1)}) %reduce-scatter.5.cloned.1.call-update) | async-done | bytes 131088 | tf_op jit(solution)/shard_map/reduce_scatter | solution.py:216
  220.9 0.9 convert_bitcast_fusion.3
  221.8 0.8 copy.95
  (185 shorter events, 1.8 us)
Async XLA Ops:
  7.2 169.2 %copy-start = (bf16[128,2048]{1,0:T(8,128)(2,1)S(1)}, bf16[128,2048]{1,0:T(8,128)(2,1)}, u32[]{:S(2)}) copy-start(bf16[128,2048]{1,0:T(8,128)(2,1)} %param.24) | copy-start | bytes 1572868
  7.2 17.1 %copy-start.2 = (bf16[256,256]{1,0:T(8,128)(2,1)S(1)}, bf16[256,256]{1,0:T(8,128)(2,1)}, u32[]{:S(2)}) copy-start(bf16[256,256]{1,0:T(8,128)(2,1)} %param.17) | copy-start | bytes 393220
  7.2 17.1 %copy-start.13 = (f32[256,2]{0,1:T(2,128)S(1)}, f32[256,2]{0,1:T(2,128)}, u32[]{:S(2)}) copy-start(f32[256,2]{0,1:T(2,128)} %param.20) | copy-start | bytes 6148
  7.2 51.6 %all-gather.6.cloned.1.call-start = ((), (), s32[]{:S(2)}) async-start(), calls=%async_computation.5 | async-start | bytes 2949120 | tf_op jit(solution)/shard_map/all_gather | solution.py:121
  24.2 69.4 %all-gather.8.cloned.1.call-start = ((), (), s32[]{:S(2)}) async-start(), calls=%async_computation.6 | async-start | bytes 2949120 | tf_op jit(solution)/shard_map/all_gather | solution.py:122
  34.1 110.8 %reduce-scatter.3.cloned.1.call-start = ((), (), s32[]{:S(2)}) async-start(), calls=%async_computation.7 | async-start | bytes 2949120 | tf_op jit(solution)/shard_map/reduce_scatter | solution.py:131
  58.8 7.2 %copy-start.8 = (bf16[1,2048,896]{2,1,0:T(8,128)(2,1)S(1)}, bf16[1,2048,896]{2,1,0:T(8,128)(2,1)}, u32[]{:S(2)}) copy-start(bf16[1,2048,896]{2,1,0:T(8,128)(2,1)} %param.22) | copy-start | bytes 11010052
  58.8 7.2 %copy-start.10 = (bf16[4,160,2048]{2,1,0:T(8,128)(2,1)S(1)}, bf16[4,160,2048]{2,1,0:T(8,128)(2,1)}, u32[]{:S(2)}) copy-start(bf16[4,160,2048]{2,1,0:T(8,128)(2,1)} %all-gather.6.cloned.1.call-done) | copy-start | bytes 7864324
  93.6 7.8 %copy-start.7 = (bf16[1,2048,896]{2,1,0:T(8,128)(2,1)S(1)}, bf16[1,2048,896]{2,1,0:T(8,128)(2,1)}, u32[]{:S(2)}) copy-start(bf16[1,2048,896]{2,1,0:T(8,128)(2,1)} %param.21) | copy-start | bytes 11010052
  101.4 3.0 %copy-start.14 = (bf16[640,896]{1,0:T(8,128)(2,1)}, bf16[640,896]{1,0:T(8,128)(2,1)S(1)}, u32[]{:S(2)}) copy-start(bf16[640,896]{1,0:T(8,128)(2,1)S(1)} %get-tuple-element.152) | copy-start | bytes 3440644
  101.4 3.0 %copy-start.18 = (bf16[640,896]{1,0:T(8,128)(2,1)}, bf16[640,896]{1,0:T(8,128)(2,1)S(1)}, u32[]{:S(2)}) copy-start(bf16[640,896]{1,0:T(8,128)(2,1)S(1)} %get-tuple-element.151) | copy-start | bytes 3440644
  101.4 2.9 %copy-start.9 = (bf16[1,2048,896]{2,1,0:T(8,128)(2,1)S(1)}, bf16[1,2048,896]{2,1,0:T(8,128)(2,1)}, u32[]{:S(2)}) copy-start(bf16[1,2048,896]{2,1,0:T(8,128)(2,1)} %param.22) | copy-start | bytes 11010052
  108.6 0.8 copy-start.4
  108.6 41.1 %copy-start.5 = (bf16[128,256]{1,0:T(8,128)(2,1)S(1)}, bf16[128,256]{1,0:T(8,128)(2,1)}, u32[]{:S(2)}) copy-start(bf16[128,256]{1,0:T(8,128)(2,1)} %param.27) | copy-start | bytes 196612
  108.6 41.2 %copy-start.6 = (bf16[128,256]{1,0:T(8,128)(2,1)S(1)}, bf16[128,256]{1,0:T(8,128)(2,1)}, u32[]{:S(2)}) copy-start(bf16[128,256]{1,0:T(8,128)(2,1)} %param.26) | copy-start | bytes 196612
  108.6 41.3 %copy-start.3 = (f32[128,256]{1,0:T(8,128)S(1)}, f32[128,256]{1,0:T(8,128)}, u32[]{:S(2)}) copy-start(f32[128,256]{1,0:T(8,128)} %param.31) | copy-start | bytes 393220
  144.9 9.2 %all-to-all-start.2 = ((bf16[4,160,256]{2,1,0:T(8,128)(2,1)}), bf16[4,160,256]{2,1,0:T(8,128)(2,1)S(1)}, u32[]{:S(2)}, u32[]{:S(2)}) async-start(bf16[4,160,256]{2,1,0:T(8,128)(2,1)} %reduce-scatter.3.cloned.1.call-done), calls=%async_computation.3 | async-start | bytes 655360 | tf_op jit(solution)/shard_map/all_to_all | solution.py:137
  148.5 27.9 %all-gather.10.cloned.1.call-start = ((), (), s32[]{:S(2)}) async-start(), calls=%async_computation.8 | async-start | bytes 1179648 | tf_op jit(solution)/shard_map/all_gather | solution.py:144
  155.1 7.5 %copy-start.15 = (bf16[640,896]{1,0:T(8,128)(2,1)S(1)}, bf16[640,896]{1,0:T(8,128)(2,1)}, u32[]{:S(2)}) copy-start(bf16[640,896]{1,0:T(8,128)(2,1)} %copy-done.14) | copy-start | bytes 3440644
  155.1 65.8 %reduce-scatter.5.cloned.1.call-start = ((), (), s32[]{:S(2)}) async-start(), calls=%async_computation.9 | async-start | bytes 655360 | tf_op jit(solution)/shard_map/reduce_scatter | solution.py:216
  155.1 7.4 %copy-start.11 = (bf16[4,160,2048]{2,1,0:T(8,128)(2,1)S(1)}, bf16[4,160,2048]{2,1,0:T(8,128)(2,1)}, u32[]{:S(2)}) copy-start(bf16[4,160,2048]{2,1,0:T(8,128)(2,1)} %all-gather.6.cloned.1.call-done) | copy-start | bytes 7864324
  162.5 4.9 %copy-start.12 = (bf16[4,160,2048]{2,1,0:T(8,128)(2,1)S(1)}, bf16[4,160,2048]{2,1,0:T(8,128)(2,1)}, u32[]{:S(2)}) copy-start(bf16[4,160,2048]{2,1,0:T(8,128)(2,1)} %all-gather.8.cloned.1.call-done) | copy-start | bytes 7864324
  162.5 4.9 %copy-start.16 = (f32[640,896]{1,0:T(8,128)S(1)}, f32[640,896]{1,0:T(8,128)}, u32[]{:S(2)}) copy-start(f32[640,896]{1,0:T(8,128)} %fusion.3) | copy-start | bytes 6881284
  162.6 4.9 %copy-start.17 = (f32[640,896]{1,0:T(8,128)S(1)}, f32[640,896]{1,0:T(8,128)}, u32[]{:S(2)}) copy-start(f32[640,896]{1,0:T(8,128)} %fusion.7) | copy-start | bytes 6881284
  178.5 16.9 %copy-start.1 = (bf16[256,2048]{1,0:T(8,128)(2,1)S(1)}, bf16[256,2048]{1,0:T(8,128)(2,1)}, u32[]{:S(2)}) copy-start(bf16[256,2048]{1,0:T(8,128)(2,1)} %all-gather.10.cloned.1.call-done) | copy-start | bytes 3145732
Sparse Core Ops, SparseCore 0:
  24.3 34.4 all-gather.5
  60.4 33.1 all-gather.7
  108.7 36.0 reduce-scatter.2
  155.2 21.1 all-gather.9
  196.9 23.9 reduce-scatter.4
where the time goes:
time: 230 us; the launch traced here: 229 us
  waiting for transfers between devices  110 us (48%)
  matrix products  52.8 us (23%)
  blocking collectives  36 us (16%)
  between operations  14.9 us (6%)
  local copies, waits for them, and re-layouts  7.07 us (3%)
  other arithmetic  4.91 us (2%)
  starting transfers between devices  3.85 us (2%)
    reduce_scatter x1, waiting for transfers between devices, local(): lax.psum_scatter(width_part.reshape(experts, capacity, full_width).astype...  34.2 us
    all_gather x1, waiting for transfers between devices, local(): lax.all_gather(part_rows, 'tp', axis=2, tiled=True)  24.6 us
    all_gather x1, waiting for transfers between devices, local(): lax.all_gather(portion_adjoint, 'tp', axis=2, tiled=True)  23.2 us
    reduce_scatter x1, waiting for transfers between devices, local(): lax.psum_scatter(lax.dot_general(full_grad, mixed, (((0,), (1,)), ((), ()...  19.8 us
    all_gather x2, blocking collectives, prefix(): pieces = jax.tree.map(lambda part: lax.all_gather(part, axis), value)  15 us
    all_to_all x1, blocking collectives, local(): lax.all_to_all(sent_rows.reshape(experts, capacity, -1), 'sp', split_axis...  11.7 us
    all_to_all x1, blocking collectives, local(): lax.all_to_all(sent_cot.reshape(experts, capacity, -1), 'sp', split_axis=...  9.32 us
    dot_general x1, matrix products, expert_work(): lax.dot_general(slot_cot, w_down, minor, preferred_element_type=jnp.float32)  7.79 us
  transfers between devices with their start and end apart: 6, of which 6 were waited for; matrix products, arithmetic and copies ran while one was open for 16% of the time, Pallas kernels for 0%

commit v1 on v0

--- a/solution.py
+++ b/solution.py
@@ -118,7 +118,7 @@
         ),
     )
     got_rows, got_cot = (
-        lax.all_gather(part_rows, "tp", axis=2, tiled=True),
+        jnp.concatenate(lax.all_gather(part_rows, "tp"), axis=2),
         lax.all_gather(portion_adjoint, "tp", axis=2, tiled=True),
     )
     full_width = got_rows.shape[2]

time: 230 us -> 230 us (level)
  local copies, waits for them, and re-layouts: 7.07 us -> 14.7 us
  waiting for transfers between devices: 110 us -> 105 us
  matrix products: 52.8 us -> 50 us
    unnamed x46 -> x55, local copies, waits for them, and re-layouts: 4.49 us -> 8.28 us
    reshape x0 -> x1, local copies, waits for them, and re-layouts: none -> 3.23 us  [local(): jnp.concatenate(lax.all_gather(part_rows, 'tp'), axis=2)]
    dot_general x1, matrix products: 7.21 us -> 4.3 us  [expert_work(): gate_act = jnp.dot(slot_rows, w_gate, preferred_element_type=jnp.float32)]
  transfers between devices with their start and end apart: 6 -> 6, of which waited for: 6 -> 6; matrix products, arithmetic and copies ran while one was open for 16% -> 17% of each run, Pallas kernels for 0% -> 0%
where the time goes in v1:
time: 230 us
  waiting for transfers between devices  105 us (46%)
  matrix products  50 us (22%)
  blocking collectives  36.1 us (16%)
  between operations  14.9 us (6%)
  local copies, waits for them, and re-layouts  14.7 us (6%)
  other arithmetic  4.89 us (2%)
  starting transfers between devices  3.79 us (2%)
    reduce_scatter x1, waiting for transfers between devices, local(): lax.psum_scatter(width_part.reshape(experts, capacity, full_width).astype...  34.3 us
    all_gather x1, waiting for transfers between devices, local(): lax.all_gather(part_rows, 'tp')  23.4 us
    all_gather x1, waiting for transfers between devices, local(): lax.all_gather(portion_adjoint, 'tp', axis=2, tiled=True)  21.3 us
    reduce_scatter x1, waiting for transfers between devices, local(): lax.psum_scatter(lax.dot_general(full_grad, mixed, (((0,), (1,)), ((), ()...  19.8 us
    all_gather x2, blocking collectives, prefix(): pieces = jax.tree.map(lambda part: lax.all_gather(part, axis), value)  15 us
    all_to_all x1, blocking collectives, local(): lax.all_to_all(sent_rows.reshape(experts, capacity, -1), 'sp', split_axis...  11.7 us
    all_to_all x1, blocking collectives, local(): lax.all_to_all(sent_cot.reshape(experts, capacity, -1), 'sp', split_axis=...  9.32 us
    unnamed x55, local copies, waits for them, and re-layouts  8.28 us
  transfers between devices with their start and end apart: 6, of which 6 were waited for; matrix products, arithmetic and copies ran while one was open for 17% of the time, Pallas kernels for 0%

profile of v1, /device:TPU:0, one launch (start us, length us, event | category | flops | bytes accessed | tf_op | source)
XLA Modules:
  0.0 229.5 jit_solution(11845344176852068890)
XLA Ops:
  7.2 0.9 copy.130
  8.1 0.1 eq.42
  8.3 0.1 eq.38
  8.4 1.2 reduce-window.6
  9.7 0.2 slice_reduce_fusion
  9.9 0.2 reduce-window.9
  10.1 0.1 add_bitcast_fusion
  10.2 0.1 reduce_sum.21
  10.3 0.1 copy.132
  10.4 0.7 add_bitcast_fusion.1
  11.1 0.3 convert_reduce_fusion
  11.3 1.1 convolution_convert_fusion.1
  12.5 11.7 %all_to_all.15 = bf16[4,160,256]{2,1,0:T(8,128)(2,1)} all-to-all(bf16[4,160,256]{2,1,0:T(8,128)(2,1)S(1)} %bitcast.112), channel_id=1, replica_groups=mesh['sp'=4,'tp'=8] {'sp'}, dimensions={0} | all-to-all | bytes 655360 | tf_op jit(solution)/shard_map/all_to_all | solution.py:113
  24.3 0.5 fusion.16
  24.8 9.3 %all_to_all.16 = bf16[4,160,256]{2,1,0:T(8,128)(2,1)} all-to-all(bf16[4,160,256]{2,1,0:T(8,128)(2,1)S(1)} %bitcast.115), channel_id=1, replica_groups=mesh['sp'=4,'tp'=8] {'sp'}, dimensions={0} | all-to-all | bytes 655360 | tf_op jit(solution)/shard_map/all_to_all | solution.py:116
  34.1 0.0 reduce-scatter.3.cloned.1.call-start
  34.2 23.4 %all-gather.11.cloned.1.call-done = bf16[32,160,256]{2,1,0:T(8,128)(2,1)} async-done(((bf16[4,160,256]{2,1,0:T(8,128)(2,1)}), bf16[32,160,256]{2,1,0:T(8,128)(2,1)}) %all-gather.11.cloned.1.call-update) | async-done | bytes 2621456 | tf_op jit(solution)/shard_map/all_gather | solution.py:121
  57.6 3.2 %copy.133 = bf16[4,160,8,256]{3,2,1,0:T(8,128)(2,1)S(1)} copy(bf16[4,160,8,256]{3,1,0,2:T(8,128)(2,1)} %bitcast.110) | data formatting | bytes 5242880 | tf_op jit(solution)/shard_map/reshape | solution.py:121
  60.9 0.9 copy.162
  61.8 1.6 copy-done.12
  63.4 4.3 %fusion.3 = f32[640,896]{1,0:T(8,128)} fusion(bf16[640,2048]{1,0:T(8,128)(2,1)S(1)} %bitcast.105, bf16[1,2048,896]{2,1,0:T(8,128)(2,1)S(1)} %copy-done.12), kind=kOutput, calls=%fused_computation.7 | convolution fusion | flops 2348810240 | bytes 8585216 | tf_op jit(solution)/shard_map/dot_general | solution.py:59
  67.7 4.3 %fusion.7 = f32[640,896]{1,0:T(8,128)} fusion(bf16[640,2048]{1,0:T(8,128)(2,1)S(1)} %bitcast.106, bf16[1,2048,896]{2,1,0:T(8,128)(2,1)S(1)} %copy-done.14), kind=kOutput, calls=%fused_computation.11 | convolution fusion | flops 2348810240 | bytes 8585216 | tf_op jit(solution)/shard_map/dot_general | solution.py:60
  71.9 21.3 %all-gather.7.cloned.1.call-done = bf16[4,160,2048]{2,1,0:T(8,128)(2,1)} async-done(((bf16[4,160,256]{2,1,0:T(8,128)(2,1)}), bf16[4,160,2048]{2,1,0:T(8,128)(2,1)}) %all-gather.7.cloned.1.call-update) | async-done | bytes 2621456 | tf_op jit(solution)/shard_map/all_gather | solution.py:122
  93.3 7.8 %multiply_convert_fusion.1 = (bf16[640,896]{1,0:T(8,128)(2,1)S(1)}, bf16[640,896]{1,0:T(8,128)(2,1)S(1)}) fusion(f32[640,896]{1,0:T(8,128)} %fusion.3, f32[640,896]{1,0:T(8,128)} %fusion.7, bf16[640,2048]{1,0:T(8,128)(2,1)} %bitcast.125, bf16[1,896,2048]{2,1,0:T(8,128)(2,1)} %param.23), kind=kOutput, calls=%fused_computation.20 | convolution fusion | flops 2356264960 | bytes 13172736 | tf_op jit(solution)/shard_map/dot_general | solution.py:64
  101.1 2.9 %fusion.1 = f32[640,2048]{1,0:T(8,128)S(1)} fusion(bf16[640,896]{1,0:T(8,128)(2,1)S(1)} %get-tuple-element.164, bf16[1,2048,896]{2,1,0:T(8,128)(2,1)S(1)} %copy-done.13), kind=kOutput, calls=%fused_computation.5 | convolution fusion | flops 2348810240 | bytes 10059776 | tf_op jit(solution)/shard_map/dot_general | solution.py:69
  104.0 4.4 %add_convert_fusion = bf16[640,2048]{1,0:T(8,128)(2,1)} fusion(f32[640,2048]{1,0:T(8,128)S(1)} %fusion.1, bf16[640,896]{1,0:T(8,128)(2,1)S(1)} %get-tuple-element.163, bf16[1,2048,896]{2,1,0:T(8,128)(2,1)S(1)} %copy-done.15), kind=kOutput, calls=%fused_computation.4 | convolution fusion | flops 2351431680 | bytes 12681216 | tf_op jit(solution)/shard_map/dot_general | solution.py:70
  108.5 0.8 copy-done.9
  109.3 0.1 copy.141
  109.4 1.0 fusion.23
  110.4 0.1 copy.140
  110.5 34.3 %reduce-scatter.3.cloned.1.call-done = bf16[4,160,256]{2,1,0:T(8,128)(2,1)} async-done(((bf16[4,160,2048]{2,1,0:T(8,128)(2,1)}), bf16[4,160,256]{2,1,0:T(8,128)(2,1)}) %reduce-scatter.3.cloned.1.call-update) | async-done | bytes 327696 | tf_op jit(solution)/shard_map/reduce_scatter | solution.py:131
  144.7 3.6 %all-to-all-start.2 = ((bf16[4,160,256]{2,1,0:T(8,128)(2,1)}), bf16[4,160,256]{2,1,0:T(8,128)(2,1)S(1)}, u32[]{:S(2)}, u32[]{:S(2)}) async-start(bf16[4,160,256]{2,1,0:T(8,128)(2,1)} %reduce-scatter.3.cloned.1.call-done), calls=%async_computation.3 | async-start | bytes 655360 | tf_op jit(solution)/shard_map/all_to_all | solution.py:137
  148.4 1.0 fusion.21
  149.4 0.7 copy.136
  150.1 0.1 copy.138
  150.2 0.7 copy.134
  151.0 0.7 copy.137
  151.7 0.8 fusion.70
  152.5 1.4 all-to-all-done.2
  153.9 1.0 fusion.17
  154.9 0.0 reduce-scatter.5.cloned.1.call-start
  155.0 7.4 %convert_bitcast_fusion.1 = bf16[1,2048,896]{2,1,0:T(8,128)(2,1)} fusion(bf16[640,2048]{1,0:T(8,128)(2,1)} %bitcast.107, bf16[640,896]{1,0:T(8,128)(2,1)} %copy-done.22), kind=kOutput, calls=%fused_computation.16 | convolution fusion | flops 2350645248 | bytes 7438336 | tf_op jit(solution)/shard_map/dot_general | solution.py:79
  162.4 4.8 %convert_bitcast_fusion.2 = bf16[1,2048,896]{2,1,0:T(8,128)(2,1)} fusion(bf16[640,2048]{1,0:T(8,128)(2,1)S(1)} %bitcast.108, bf16[640,896]{1,0:T(8,128)(2,1)S(1)} %copy-done.19), kind=kOutput, calls=%fused_computation.17 | convolution fusion | flops 2350645248 | bytes 7438336 | tf_op jit(solution)/shard_map/dot_general | solution.py:76
  167.3 4.6 %convert_bitcast_fusion = bf16[1,896,2048]{2,1,0:T(8,128)(2,1)} fusion(bf16[640,2048]{1,0:T(8,128)(2,1)S(1)} %bitcast.126, f32[640,896]{1,0:T(8,128)S(1)} %copy-done.21, f32[640,896]{1,0:T(8,128)S(1)} %copy-done.20), kind=kOutput, calls=%fused_computation.15 | convolution fusion | flops 2354085888 | bytes 10878976 | tf_op jit(solution)/shard_map/dot_general | solution.py:82
  171.9 4.8 %all-gather.9.cloned.1.call-done = bf16[256,2048]{1,0:T(8,128)(2,1)} async-done(((bf16[256,256]{1,0:T(8,128)(2,1)}), bf16[256,2048]{1,0:T(8,128)(2,1)}) %all-gather.9.cloned.1.call-update) | async-done | bytes 1048592 | tf_op jit(solution)/shard_map/all_gather | solution.py:144
  176.7 1.8 fusion.40
  180.6 7.1 %all-gather.1 = f32[512,1]{0,1:T(1,128)S(1)} all-gather(f32[128,1]{0,1:T(1,128)S(1)} %get-tuple-element.168), channel_id=3, replica_groups=mesh['sp'=4,'tp'=8] {'sp'}, dimensions={0}, use_global_device_ids=true | all-gather | bytes 2560 | tf_op jit(solution)/shard_map/all_gather | solution.py:13
  187.8 7.9 %all-gather.2 = f32[512,1]{0,1:T(1,128)S(1)} all-gather(f32[128,1]{0,1:T(1,128)S(1)} %get-tuple-element.167), channel_id=4, replica_groups=mesh['sp'=4,'tp'=8] {'sp'}, dimensions={0}, use_global_device_ids=true | all-gather | bytes 2560 | tf_op jit(solution)/shard_map/all_gather | solution.py:13
  195.7 1.4 convolution_convert_fusion
  197.2 0.1 while.14
  197.3 0.1 rev.16
  197.4 0.1 rev.15
  197.5 0.2 fusion.43
  197.7 0.1 copy.146
  197.8 0.9 fusion.62
  198.7 0.1 copy.148
  198.8 0.1 copy.151
  199.0 0.9 fusion.59
  199.9 0.1 copy.153
  200.0 0.7 copy.155
  200.7 0.7 copy.156
  201.5 19.8 %reduce-scatter.5.cloned.1.call-done = bf16[512,128]{1,0:T(8,128)(2,1)} async-done(((bf16[2048,128]{1,0:T(8,128)(2,1)}), bf16[512,128]{1,0:T(8,128)(2,1)}) %reduce-scatter.5.cloned.1.call-update) | async-done | bytes 131088 | tf_op jit(solution)/shard_map/reduce_scatter | solution.py:216
  221.2 0.9 convert_bitcast_fusion.3
  222.2 0.8 copy.154
  (195 shorter events, 1.9 us)
Async XLA Ops:
  7.2 169.6 %copy-start = (bf16[128,2048]{1,0:T(8,128)(2,1)S(1)}, bf16[128,2048]{1,0:T(8,128)(2,1)}, u32[]{:S(2)}) copy-start(bf16[128,2048]{1,0:T(8,128)(2,1)} %param.24) | copy-start | bytes 1572868
  7.2 17.1 %copy-start.4 = (bf16[256,256]{1,0:T(8,128)(2,1)S(1)}, bf16[256,256]{1,0:T(8,128)(2,1)}, u32[]{:S(2)}) copy-start(bf16[256,256]{1,0:T(8,128)(2,1)} %param.17) | copy-start | bytes 393220
  7.2 17.1 %copy-start.17 = (f32[256,2]{0,1:T(2,128)S(1)}, f32[256,2]{0,1:T(2,128)}, u32[]{:S(2)}) copy-start(f32[256,2]{0,1:T(2,128)} %param.20) | copy-start | bytes 6148
  7.2 50.4 %all-gather.11.cloned.1.call-start = ((), (), s32[]{:S(2)}) async-start(), calls=%async_computation.9 | async-start | bytes 2949120 | tf_op jit(solution)/shard_map/all_gather | solution.py:121
  24.2 69.0 %all-gather.7.cloned.1.call-start = ((), (), s32[]{:S(2)}) async-start(), calls=%async_computation.5 | async-start | bytes 2949120 | tf_op jit(solution)/shard_map/all_gather | solution.py:122
  34.1 110.6 %reduce-scatter.3.cloned.1.call-start = ((), (), s32[]{:S(2)}) async-start(), calls=%async_computation.6 | async-start | bytes 2949120 | tf_op jit(solution)/shard_map/reduce_scatter | solution.py:131
  60.8 2.5 %copy-start.12 = (bf16[1,2048,896]{2,1,0:T(8,128)(2,1)S(1)}, bf16[1,2048,896]{2,1,0:T(8,128)(2,1)}, u32[]{:S(2)}) copy-start(bf16[1,2048,896]{2,1,0:T(8,128)(2,1)} %param.21) | copy-start | bytes 11010052
  61.7 5.9 %copy-start.1 = (bf16[80,8,8,256]{3,1,2,0:T(8,128)(2,1)}, bf16[80,8,8,256]{3,1,2,0:T(8,128)(2,1)S(1)}, u32[]{:S(2)}) copy-start(bf16[80,8,8,256]{3,1,2,0:T(8,128)(2,1)S(1)} %copy.162) | copy-start | bytes 7864324
  63.4 4.3 %copy-start.14 = (bf16[1,2048,896]{2,1,0:T(8,128)(2,1)S(1)}, bf16[1,2048,896]{2,1,0:T(8,128)(2,1)}, u32[]{:S(2)}) copy-start(bf16[1,2048,896]{2,1,0:T(8,128)(2,1)} %param.22) | copy-start | bytes 11010052
  93.3 7.8 %copy-start.13 = (bf16[1,2048,896]{2,1,0:T(8,128)(2,1)S(1)}, bf16[1,2048,896]{2,1,0:T(8,128)(2,1)}, u32[]{:S(2)}) copy-start(bf16[1,2048,896]{2,1,0:T(8,128)(2,1)} %param.21) | copy-start | bytes 11010052
  101.1 3.0 %copy-start.18 = (bf16[640,896]{1,0:T(8,128)(2,1)}, bf16[640,896]{1,0:T(8,128)(2,1)S(1)}, u32[]{:S(2)}) copy-start(bf16[640,896]{1,0:T(8,128)(2,1)S(1)} %get-tuple-element.164) | copy-start | bytes 3440644
  101.1 3.0 %copy-start.22 = (bf16[640,896]{1,0:T(8,128)(2,1)}, bf16[640,896]{1,0:T(8,128)(2,1)S(1)}, u32[]{:S(2)}) copy-start(bf16[640,896]{1,0:T(8,128)(2,1)S(1)} %get-tuple-element.163) | copy-start | bytes 3440644
  101.1 2.9 %copy-start.15 = (bf16[1,2048,896]{2,1,0:T(8,128)(2,1)S(1)}, bf16[1,2048,896]{2,1,0:T(8,128)(2,1)}, u32[]{:S(2)}) copy-start(bf16[1,2048,896]{2,1,0:T(8,128)(2,1)} %param.22) | copy-start | bytes 11010052
  108.4 0.8 copy-start.9
  108.4 41.7 %copy-start.10 = (bf16[128,256]{1,0:T(8,128)(2,1)S(1)}, bf16[128,256]{1,0:T(8,128)(2,1)}, u32[]{:S(2)}) copy-start(bf16[128,256]{1,0:T(8,128)(2,1)} %param.27) | copy-start | bytes 196612
  108.4 41.8 %copy-start.11 = (bf16[128,256]{1,0:T(8,128)(2,1)S(1)}, bf16[128,256]{1,0:T(8,128)(2,1)}, u32[]{:S(2)}) copy-start(bf16[128,256]{1,0:T(8,128)(2,1)} %param.26) | copy-start | bytes 196612
  108.4 42.5 %copy-start.7 = (f32[128,256]{1,0:T(8,128)S(1)}, f32[128,256]{1,0:T(8,128)}, u32[]{:S(2)}) copy-start(f32[128,256]{1,0:T(8,128)} %param.31) | copy-start | bytes 393220
  144.7 9.2 %all-to-all-start.2 = ((bf16[4,160,256]{2,1,0:T(8,128)(2,1)}), bf16[4,160,256]{2,1,0:T(8,128)(2,1)S(1)}, u32[]{:S(2)}, u32[]{:S(2)}) async-start(bf16[4,160,256]{2,1,0:T(8,128)(2,1)} %reduce-scatter.3.cloned.1.call-done), calls=%async_computation.3 | async-start | bytes 655360 | tf_op jit(solution)/shard_map/all_to_all | solution.py:137
  148.4 28.4 %all-gather.9.cloned.1.call-start = ((), (), s32[]{:S(2)}) async-start(), calls=%async_computation.7 | async-start | bytes 1179648 | tf_op jit(solution)/shard_map/all_gather | solution.py:144
  154.9 7.5 %copy-start.2 = (bf16[80,8,8,256]{3,1,2,0:T(8,128)(2,1)S(1)}, bf16[80,8,8,256]{3,1,2,0:T(8,128)(2,1)}, u32[]{:S(2)}) copy-start(bf16[80,8,8,256]{3,1,2,0:T(8,128)(2,1)} %copy-done.1) | copy-start | bytes 7864324
  154.9 66.3 %reduce-scatter.5.cloned.1.call-start = ((), (), s32[]{:S(2)}) async-start(), calls=%async_computation.8 | async-start | bytes 655360 | tf_op jit(solution)/shard_map/reduce_scatter | solution.py:216
  155.0 7.4 %copy-start.19 = (bf16[640,896]{1,0:T(8,128)(2,1)S(1)}, bf16[640,896]{1,0:T(8,128)(2,1)}, u32[]{:S(2)}) copy-start(bf16[640,896]{1,0:T(8,128)(2,1)} %copy-done.18) | copy-start | bytes 3440644
  162.4 4.9 %copy-start.16 = (bf16[4,160,2048]{2,1,0:T(8,128)(2,1)S(1)}, bf16[4,160,2048]{2,1,0:T(8,128)(2,1)}, u32[]{:S(2)}) copy-start(bf16[4,160,2048]{2,1,0:T(8,128)(2,1)} %all-gather.7.cloned.1.call-done) | copy-start | bytes 7864324
  162.4 4.9 %copy-start.20 = (f32[640,896]{1,0:T(8,128)S(1)}, f32[640,896]{1,0:T(8,128)}, u32[]{:S(2)}) copy-start(f32[640,896]{1,0:T(8,128)} %fusion.3) | copy-start | bytes 6881284
  162.4 4.9 %copy-start.21 = (f32[640,896]{1,0:T(8,128)S(1)}, f32[640,896]{1,0:T(8,128)}, u32[]{:S(2)}) copy-start(f32[640,896]{1,0:T(8,128)} %fusion.7) | copy-start | bytes 6881284
  167.3 9.5 %copy-start.5 = (f32[128,256]{0,1:T(8,128)S(1)}, f32[128,256]{0,1:T(8,128)}, u32[]{:S(2)}) copy-start(f32[128,256]{0,1:T(8,128)} %copy.136) | copy-start | bytes 393220
  167.3 9.5 %copy-start.6 = (bf16[128,256]{0,1:T(8,128)(2,1)S(1)}, bf16[128,256]{0,1:T(8,128)(2,1)}, u32[]{:S(2)}) copy-start(bf16[128,256]{0,1:T(8,128)(2,1)} %copy.134) | copy-start | bytes 196612
  167.3 9.5 %copy-start.8 = (f32[128,256]{0,1:T(8,128)S(1)}, f32[128,256]{0,1:T(8,128)}, u32[]{:S(2)}) copy-start(f32[128,256]{0,1:T(8,128)} %copy.137) | copy-start | bytes 393220
  178.9 16.9 %copy-start.3 = (bf16[256,2048]{1,0:T(8,128)(2,1)S(1)}, bf16[256,2048]{1,0:T(8,128)(2,1)}, u32[]{:S(2)}) copy-start(bf16[256,2048]{1,0:T(8,128)(2,1)} %all-gather.9.cloned.1.call-done) | copy-start | bytes 3145732
Sparse Core Ops, SparseCore 0:
  24.3 33.2 all-gather.10
  59.2 34.0 all-gather.6
  108.6 36.1 reduce-scatter.2
  155.0 21.6 all-gather.8
  197.3 23.9 reduce-scatter.4
